TPU v7x, 128 devices: a whole 4x4x4 slice. The times are simulated.
128 devices in a mesh: sp: 64 (over z, y, x), tp: 2 (over core).
Axes of the slice: x: 4, y: 4, z: 4, core: 2. Of those that a mesh axis runs over, the one named last changes fastest.
Arguments:
- tokens: bfloat16 [32768, 4096], P(('sp', 'tp')), may hold values from -6 to 6
- norm_gain: float32 [4096], replicated, may hold values from 0.5 to 1.5
- query_weight: bfloat16 [4096, 1024], P(None, 'tp'), may hold values from -0.09375 to 0.09375
- key_weight: bfloat16 [4096, 1024], P(None, 'tp'), may hold values from -0.09375 to 0.09375
- value_weight: bfloat16 [4096, 2048], P(None, 'tp'), may hold values from -0.09375 to 0.09375
- gate_weight: bfloat16 [4096, 2048], P(None, 'tp'), may hold values from -0.09375 to 0.09375
- decay_bias: float32 [1024], P('tp'), may hold values from -0.5 to 0.5
- head_gain: float32 [2048], P('tp'), may hold values from 0.5 to 1.5
- out_weight: bfloat16 [2048, 4096], P('tp'), may hold values from -0.125 to 0.125
Outputs:
- layer_out: bfloat16 [32768, 4096], P(('sp', 'tp'))
All inputs are finite; a program needn't handle non-finite values.
Results may differ from a plain program's by a relative error of at most 0.015.
Values may be sent and summed in bfloat16 or wider, within the bound.
A program may use at most 192 MiB of HBM per device.

v0:
```python
import functools
import math

import jax
import jax.numpy as jnp
from jax import lax
from jax.experimental import pallas as pl
from jax.experimental.pallas import tpu as pltpu
from jax.sharding import PartitionSpec as P

HEAD_K = 128
HEAD_V = 256

epsilon = 1e-06
decay_power = 16.0
MESH = pl.DeviceIdType.MESH
f32 = jnp.float32
bf16 = jnp.bfloat16
OUT_TILE = 512
VMEM_BYTES = 67_000_000


def nn(a, b):
    return jnp.dot(a, b, preferred_element_type=f32)


def nt(a, b):
    return lax.dot_general(a, b, (((1,), (1,)), ((), ())), preferred_element_type=f32)


def tn(a, b):
    return lax.dot_general(a, b, (((0,), (0,)), ((), ())), preferred_element_type=f32)


def kernel(
    sp_count,
    tokens,
    norm_gain,
    wq,
    wk,
    wv,
    wg,
    decay_bias,
    head_gain,
    wo,
    out,
    xn,
    w,
    wout,
    y,
    kin,
    qin,
    pv,
    gated,
    st_send,
    st_recv,
    tot_send,
    tot_recv,
    acc,
    c_send,
    c_recv,
    o_send,
    o_recv,
    o_buf,
    tok_sem,
    w_sem,
    wo_sem,
    tok_send,
    tok_recv,
    a_send,
    a_recv,
    b_send,
    b_recv,
    cs_send,
    cs_recv,
    os_send,
    os_recv,
    ob_sem,
):
    s = lax.axis_index("sp")
    c = lax.axis_index("tp")
    other = 1 - c
    half = tokens.shape[0]
    span = 2 * half
    width = wk.shape[1]
    heads = width // HEAD_K
    per = width // HEAD_V
    vtiles = wv.shape[1] // width
    inner = heads
    groups = sp_count // inner
    g = s // inner
    j = lax.rem(s, inner)

    own = pl.ds(pl.multiple_of(c * half, half), half)
    theirs = pl.ds(pl.multiple_of(other * half, half), half)

    def inner_dev(i):
        return {"sp": g * inner + i, "tp": c}

    def group_dev(k):
        return {"sp": k * inner + j, "tp": c}

    local_tok = pltpu.make_async_copy(tokens, xn.at[own], tok_sem)
    local_tok.start()
    sources = [wk.at[:, :]]
    sources += [wv.at[:, pl.ds(t * width, width)] for t in range(vtiles)]
    sources += [wq.at[:, :]]
    sources += [wg.at[:, pl.ds(t * width, width)] for t in range(vtiles)]
    count = len(sources)
    pltpu.make_async_copy(sources[0], w.at[0], w_sem.at[0]).start()

    barrier = pltpu.get_barrier_semaphore()
    pl.semaphore_signal(barrier, inc=1, device_id={"sp": s, "tp": other}, device_id_type=MESH)
    for d in range(1, inner):
        pl.semaphore_signal(
            barrier, inc=1, device_id=inner_dev(lax.rem(j + d, inner)), device_id_type=MESH
        )
    for d in range(1, groups):
        pl.semaphore_signal(
            barrier, inc=1, device_id=group_dev(lax.rem(g + d, groups)), device_id_type=MESH
        )
    pl.semaphore_wait(barrier, inner + groups - 1)

    send_tok = pltpu.make_async_remote_copy(
        src_ref=tokens,
        dst_ref=xn.at[own],
        send_sem=tok_send,
        recv_sem=tok_recv,
        device_id={"sp": s, "tp": other},
        device_id_type=MESH,
    )
    send_tok.start()
    for t in range(1, count):
        pltpu.make_async_copy(sources[t], w.at[t], w_sem.at[t]).start()
    wo_copy = pltpu.make_async_copy(wo, wout, wo_sem)
    wo_copy.start()

    chunk = 16

    def norm_rows(first):
        @pl.loop(0, half // chunk)
        def _(i):
            rows = pl.ds(pl.multiple_of(first + i * chunk, chunk), chunk)
            x = xn[rows, :].astype(f32)
            scale = lax.rsqrt(jnp.mean(x * x, axis=-1, keepdims=True) + epsilon)
            xn[rows, :] = (x * scale * norm_gain[...]).astype(bf16)

    def wait_w(t):
        pltpu.make_async_copy(wk, w.at[t], w_sem.at[t]).wait()

    local_tok.wait()
    norm_rows(c * half)
    wait_w(0)
    y[0, own, :] = nn(xn[own, :], w[0]).astype(bf16)
    send_tok.wait()
    norm_rows(other * half)
    y[0, theirs, :] = nn(xn[theirs, :], w[0]).astype(bf16)

    def project(t):
        wait_w(t)
        y[t] = nn(xn[...], w[t]).astype(bf16)

    @pl.loop(1, 1 + vtiles)
    def _(t):
        project(t)

    def log_decay_of(bias):
        return -jnp.log1p(jnp.exp(-(bias + math.log(sp_count * span / 8.0)))) / decay_power

    steps = (lax.broadcasted_iota(jnp.int32, (span, HEAD_K), 0) + 1).astype(f32)

    def column(row):
        half_tile = jnp.broadcast_to(row, (HEAD_K, HEAD_K)).T
        return jnp.concatenate([half_tile] * (HEAD_V // HEAD_K), axis=1)

    def value_of(h):
        return y[1 + h // per, :, pl.ds((h % per) * HEAD_V, HEAD_V)]

    for h in range(heads):
        keys = pl.ds(h * HEAD_K, HEAD_K)
        row = log_decay_of(decay_bias[pl.ds(h, 1), :])
        k_here = (y[0, :, keys].astype(f32) * jnp.exp(-row * steps)).astype(bf16)
        kin[:, keys] = k_here
        st_send[h] = (tn(k_here, value_of(h)) * column(jnp.exp(row * span))).astype(bf16)

    def copies(src, dst, ssem, rsem):
        made = []
        for d in range(1, inner):
            i = lax.rem(j + d, inner)
            made.append(
                pltpu.make_async_remote_copy(
                    src_ref=src.at[i],
                    dst_ref=dst.at[j],
                    send_sem=ssem.at[d - 1],
                    recv_sem=rsem.at[d - 1],
                    device_id=inner_dev(i),
                    device_id_type=MESH,
                )
            )
        return made

    a_copies = copies(st_send, st_recv, a_send, a_recv)
    for copy in a_copies:
        copy.start()
    st_recv[j] = st_send[j]

    @pl.loop(1 + vtiles, 3 + vtiles)
    def _(t):
        project(t)

    for copy in a_copies:
        copy.wait()
    mine = log_decay_of(decay_bias[pl.ds(j, 1), :])
    step_decay = column(jnp.exp(mine * span))
    total = st_recv[0].astype(f32)
    for i in range(1, inner):
        total = total * step_decay + st_recv[i].astype(f32)
    tot_send[...] = total.astype(bf16)

    def b_copy(d):
        return pltpu.make_async_remote_copy(
            src_ref=tot_send,
            dst_ref=tot_recv.at[d - 1],
            send_sem=b_send.at[d - 1],
            recv_sem=b_recv.at[d - 1],
            device_id=group_dev(lax.rem(g + d, groups)),
            device_id_type=MESH,
        )

    for d in range(1, groups):

        @pl.when(g + d < groups)
        def _():
            b_copy(d).start()

    @pl.loop(3 + vtiles, count)
    def _(t):
        project(t)

    for h in range(heads):
        keys = pl.ds(h * HEAD_K, HEAD_K)
        values = pl.ds(h * HEAD_V, HEAD_V)
        row = log_decay_of(decay_bias[pl.ds(h, 1), :])
        q_here = (
            y[1 + vtiles, :, keys].astype(f32) * (jnp.exp(row * steps) * HEAD_K ** (-0.5))
        ).astype(bf16)
        qin[:, keys] = q_here
        v_here = value_of(h)
        parts = 2
        rows = span // parts
        for p in range(parts):
            last = (p + 1) * rows
            scores = nt(q_here[p * rows : last], kin[pl.ds(0, last), keys])
            at = lax.broadcasted_iota(jnp.int32, scores.shape, 0) + p * rows
            to = lax.broadcasted_iota(jnp.int32, scores.shape, 1)
            scores = jnp.where(to <= at, scores, 0.0).astype(bf16)
            pv[pl.ds(p * rows, rows), values] = nn(scores, v_here[:last])

    acc[...] = jnp.zeros_like(acc)
    for d in range(1, groups):

        @pl.when(g >= d)
        def _():
            b_copy(d).wait_recv()
            far = column(jnp.exp(mine * (span * inner * (d - 1))))
            acc[...] += tot_recv[d - 1].astype(f32) * far

    carry = acc[...]
    c_send[0] = carry.astype(bf16)
    for i in range(1, inner):
        carry = carry * step_decay + st_recv[i - 1].astype(f32)
        c_send[i] = carry.astype(bf16)
    c_copies = copies(c_send, c_recv, cs_send, cs_recv)
    for copy in c_copies:
        copy.start()
    c_recv[j] = c_send[j]
    for copy in c_copies:
        copy.wait()

    for h in range(heads):
        keys = pl.ds(h * HEAD_K, HEAD_K)
        values = pl.ds(h * HEAD_V, HEAD_V)
        att = pv[:, values] + nn(qin[:, keys], c_recv[h])
        scale = lax.rsqrt(jnp.mean(att * att, axis=-1, keepdims=True) + epsilon)
        u = y[2 + vtiles + h // per, :, pl.ds((h % per) * HEAD_V, HEAD_V)].astype(f32)
        silu = u / (1.0 + jnp.exp(-u))
        gated[:, values] = (att * scale * head_gain[:, values] * silu).astype(bf16)

    tiles = wout.shape[1] // OUT_TILE

    def o_copy(t):
        return pltpu.make_async_remote_copy(
            src_ref=o_send.at[t],
            dst_ref=o_recv.at[t],
            send_sem=os_send.at[t],
            recv_sem=os_recv.at[t],
            device_id={"sp": s, "tp": other},
            device_id_type=MESH,
        )

    def out_copy(t):
        columns = pl.ds(pl.multiple_of(t * OUT_TILE, OUT_TILE), OUT_TILE)
        return pltpu.make_async_copy(o_buf.at[t], out.at[:, columns], ob_sem.at[t])

    wo_copy.wait()

    @pl.loop(0, tiles)
    def _(t):
        columns = pl.ds(pl.multiple_of(t * OUT_TILE, OUT_TILE), OUT_TILE)
        o_send[t] = nn(gated[theirs, :], wout[:, columns]).astype(bf16)
        o_copy(t).start()

    @pl.loop(0, tiles)
    def _(t):
        columns = pl.ds(pl.multiple_of(t * OUT_TILE, OUT_TILE), OUT_TILE)
        part = nn(gated[own, :], wout[:, columns])
        o_copy(t).wait()
        o_buf[t] = (part + o_recv[t].astype(f32)).astype(bf16)
        out_copy(t).start()

    @pl.loop(0, tiles)
    def _(t):
        out_copy(t).wait()

    for d in range(1, groups):

        @pl.when(g + d < groups)
        def _():
            b_copy(d).wait_send()


def per_device(sp_count, tokens, norm_gain, wq, wk, wv, wg, decay_bias, head_gain, wo):
    half, model = tokens.shape
    span = 2 * half
    width = wk.shape[1]
    vwidth = wv.shape[1]
    vtiles = vwidth // width
    heads = width // HEAD_K
    groups = sp_count // heads
    count = 2 + 2 * vtiles
    tiles = model // OUT_TILE
    state = (HEAD_K, HEAD_V)
    vm = pltpu.VMEM
    dma = pltpu.SemaphoreType.DMA
    hbm = pl.BlockSpec(memory_space=pltpu.HBM)
    vmem = pl.BlockSpec(memory_space=pltpu.VMEM)
    return pl.pallas_call(
        functools.partial(kernel, sp_count),
        out_shape=jax.ShapeDtypeStruct((half, model), bf16),
        in_specs=[hbm, vmem, hbm, hbm, hbm, hbm, vmem, vmem, hbm],
        out_specs=hbm,
        scratch_shapes=[
            vm((span, model), bf16),
            vm((count, model, width), bf16),
            vm((vwidth, model), bf16),
            vm((count, span, width), bf16),
            vm((span, width), bf16),
            vm((span, width), bf16),
            vm((span, vwidth), f32),
            vm((span, vwidth), bf16),
            vm((heads,) + state, bf16),
            vm((heads,) + state, bf16),
            vm(state, bf16),
            vm((groups,) + state, bf16),
            vm(state, f32),
            vm((heads,) + state, bf16),
            vm((heads,) + state, bf16),
            vm((tiles, half, OUT_TILE), bf16),
            vm((tiles, half, OUT_TILE), bf16),
            vm((tiles, half, OUT_TILE), bf16),
            dma,
            dma((count,)),
            dma,
            dma,
            dma,
            dma((heads,)),
            dma((heads,)),
            dma((groups,)),
            dma((groups,)),
            dma((heads,)),
            dma((heads,)),
            dma((tiles,)),
            dma((tiles,)),
            dma((tiles,)),
        ],
        compiler_params=pltpu.CompilerParams(
            collective_id=0, has_side_effects=True, vmem_limit_bytes=VMEM_BYTES
        ),
    )(
        tokens,
        norm_gain.reshape(1, model),
        wq,
        wk,
        wv,
        wg,
        decay_bias.reshape(heads, HEAD_K),
        head_gain.reshape(1, vwidth),
        wo,
    )


def solution(mesh):
    return jax.shard_map(
        functools.partial(per_device, mesh.shape["sp"]),
        mesh=mesh,
        in_specs=(
            P(("sp", "tp"), None),
            P(),
            P(None, "tp"),
            P(None, "tp"),
            P(None, "tp"),
            P(None, "tp"),
            P("tp"),
            P("tp"),
            P("tp", None),
        ),
        out_specs=P(("sp", "tp"), None),
        check_vma=False,
    )
```

profile of v0, /device:TPU:120, one launch (start us, length us, event | category | flops | bytes accessed | tf_op | source)
XLA Modules:
  0.0 59.2 jit_solution(9680145178705171583)
XLA Ops:
  0.0 56.0 %shard_map.91 = bf16[256,4096]{1,0:T(8,128)(2,1)} custom-call(bf16[256,4096]{1,0:T(8,128)(2,1)} %tokens.1, f32[1,4096]{1,0:T(1,128)} %bitcast.3, bf16[4096,512]{1,0:T(8,128)(2,1)} %wq.1, bf16[4096,512]{1,0:T(8,128)(2,1)} %wk.1, bf16[4096,1024]{1,0:T(8,128)(2,1)} %wv.1, bf16[4096,1024]{1,0:T(8,128)(2,1)} %wg.1, f32[4,128]{1,0:T(4,128)} %bitcast.5, ...), custom_call_target="tpu_custom_call" | custom-call | tf_op jit(solution)/shard_map/pallas_call | solution.py:347
  56.0 3.1 %copy.11 = bf16[256,4096]{1,0:T(8,128)(2,1)} copy(bf16[256,4096]{1,0:T(8,128)(2,1)} %shard_map.91) | data formatting | bytes 4194304
where the time goes:
time: 59.4 us; the launch traced here: 59.2 us
  Pallas kernels  56 us (94%)
  local copies, waits for them, and re-layouts  3.13 us (5%)
    pallas_call x1, Pallas kernels, per_device(): pl.pallas_call(functools.partial(kernel, sp_count), out_shape=jax.ShapeDt...  56 us
    unnamed x1, local copies, waits for them, and re-layouts  3.13 us

commit v1 on v0

v1 whole, which is shorter than its diff:
```python
import functools
import math
import types

import jax
import jax.numpy as jnp
from jax import lax
from jax.experimental import pallas as pl
from jax.experimental.pallas import tpu as pltpu
from jax.sharding import PartitionSpec as P

HEAD_K = 128
HEAD_V = 256
PIECES = 16
PIECE_ROWS = 16
LANES = 128

epsilon = 1e-06
decay_power = 16.0
MESH = pl.DeviceIdType.MESH
f32 = jnp.float32
bf16 = jnp.bfloat16
OUT_TILE = 512
TOKEN_CHUNKS = 4
VMEM_BYTES = 67_000_000


def nn(a, b):
    return jnp.dot(a, b, preferred_element_type=f32)


def nt(a, b):
    return lax.dot_general(a, b, (((1,), (1,)), ((), ())), preferred_element_type=f32)


def tn(a, b):
    return lax.dot_general(a, b, (((0,), (0,)), ((), ())), preferred_element_type=f32)


def mark(name):
    pass


def kernel(sp_count, names, *refs):
    r = types.SimpleNamespace(**dict(zip(names, refs, strict=True)))
    s = lax.axis_index("sp")
    c = lax.axis_index("tp")
    other = 1 - c
    half, model = r.tokens.shape
    span = 2 * half
    heads = r.wk.shape[1] // HEAD_K
    groups = 2
    pair = heads // groups
    vcols = pair * HEAD_V
    inner = PIECES
    outer = sp_count // inner
    z = s // inner
    p = lax.rem(s, inner)

    own = pl.ds(pl.multiple_of(c * half, half), half)
    theirs = pl.ds(pl.multiple_of(other * half, half), half)
    partner = {"sp": s, "tp": other}

    def plane_dev(i):
        return {"sp": z * inner + i, "tp": c}

    def outer_dev(k):
        return {"sp": k * inner + p, "tp": c}

    def remote(src, dst, ssem, rsem, device):
        return pltpu.make_async_remote_copy(
            src_ref=src,
            dst_ref=dst,
            send_sem=ssem,
            recv_sem=rsem,
            device_id=device,
            device_id_type=MESH,
        )

    chunk = half // TOKEN_CHUNKS
    tok_copies = []
    for i in range(TOKEN_CHUNKS):
        rows = pl.ds(i * chunk, chunk)
        mine = pl.ds(pl.multiple_of(c * half + i * chunk, chunk), chunk)
        tok_copies.append(
            pltpu.make_async_copy(r.tokens.at[rows, :], r.xn.at[mine, :], r.tok_sem.at[i])
        )
    small = [
        pltpu.make_async_copy(r.norm_gain, r.gain_v, r.small_sem.at[0]),
        pltpu.make_async_copy(r.decay_bias, r.bias_v, r.small_sem.at[1]),
        pltpu.make_async_copy(r.head_gain, r.hgain_v, r.small_sem.at[2]),
    ]
    wk_copy = pltpu.make_async_copy(r.wk, r.wk_v, r.w_sem.at[0])
    wq_copy = pltpu.make_async_copy(r.wq, r.wq_v, r.w_sem.at[1])
    wv_copies, wg_copies = [], []
    for g in range(groups):
        cols = pl.ds(g * vcols, vcols)
        wv_copies.append(
            pltpu.make_async_copy(r.wv.at[:, cols], r.wv_v.at[:, cols], r.w_sem.at[2 + g])
        )
        wg_copies.append(
            pltpu.make_async_copy(
                r.wg.at[:, cols], r.wg_v.at[:, cols], r.w_sem.at[2 + groups + g]
            )
        )
    wo_copy = pltpu.make_async_copy(r.wo, r.wo_v, r.wo_sem)
    tok_copies[0].start()
    small[0].start()
    for copy in tok_copies[1:]:
        copy.start()
    for copy in [wk_copy] + wv_copies + [wq_copy] + small[1:] + wg_copies + [wo_copy]:
        copy.start()

    barrier = pltpu.get_barrier_semaphore()
    pl.semaphore_signal(barrier, inc=1, device_id=partner, device_id_type=MESH)
    for d in range(1, inner):
        pl.semaphore_signal(
            barrier, inc=1, device_id=plane_dev(lax.rem(p + d, inner)), device_id_type=MESH
        )
    for d in range(1, outer):
        pl.semaphore_signal(
            barrier, inc=1, device_id=outer_dev(lax.rem(z + d, outer)), device_id_type=MESH
        )

    mark("p_norm")
    sub = 16
    small[0].wait()
    for i in range(TOKEN_CHUNKS):
        tok_copies[i].wait()
        first = c * half + i * chunk

        @pl.loop(0, chunk // sub, unroll=True)
        def _(k):
            rows = pl.ds(pl.multiple_of(first + k * sub, sub), sub)
            x = r.xn[rows, :].astype(f32)
            scale = lax.rsqrt(jnp.mean(x * x, axis=-1, keepdims=True) + epsilon)
            r.scale_v[pl.ds(k * sub, sub), :] = jnp.broadcast_to(scale, (sub, LANES))

        @pl.loop(0, chunk // sub)
        def _(k):
            rows = pl.ds(pl.multiple_of(first + k * sub, sub), sub)
            x = r.xn[rows, :].astype(f32)
            scale = r.scale_v[pl.ds(pl.multiple_of(k * sub, sub), sub), pl.ds(0, 1)]
            r.xn[rows, :] = (x * scale * r.gain_v[...]).astype(bf16)

    mark("p_barrier")
    pl.semaphore_wait(barrier, inner + outer - 1)
    send_tok = remote(r.xn.at[own, :], r.xn.at[own, :], r.tok_send, r.tok_recv, partner)
    send_tok.start()

    mark("p_kown")
    wk_copy.wait()
    r.yk[own, :] = nn(r.xn[own, :], r.wk_v[...]).astype(bf16)
    mark("p_vown")
    for copy in wv_copies:
        copy.wait()
    r.yv[own, :] = nn(r.xn[own, :], r.wv_v[...]).astype(bf16)
    mark("p_qown")
    wq_copy.wait()
    r.yq[own, :] = nn(r.xn[own, :], r.wq_v[...]).astype(bf16)
    mark("p_waittok")
    for copy in small[1:]:
        copy.wait()
    send_tok.wait()

    def log_decay_of(bias):
        return -jnp.log1p(jnp.exp(-(bias + math.log(sp_count * span / 8.0)))) / decay_power

    steps = (lax.broadcasted_iota(jnp.int32, (span, HEAD_K), 0) + (s * span + 1)).astype(f32)

    def values_of(h):
        return pl.ds(h * HEAD_V, HEAD_V)

    def keys_of(h):
        return pl.ds(h * HEAD_K, HEAD_K)

    mark("p_ktheir")
    r.yk[theirs, :] = nn(r.xn[theirs, :], r.wk_v[...]).astype(bf16)
    for h in range(heads):
        row = log_decay_of(r.bias_v[pl.ds(h, 1), :])
        r.kin[:, keys_of(h)] = (r.yk[:, keys_of(h)].astype(f32) * jnp.exp(-row * steps)).astype(
            bf16
        )

    def send_states(g):
        for d in range(1, inner):
            i = lax.rem(p + d, inner)
            remote(
                r.st_send.at[g, i], r.st_recv.at[g, d], r.a_send.at[g], r.a_recv.at[g], plane_dev(i)
            ).start()
        r.st_recv[g, 0] = r.st_send[g, p]

    for g in range(groups):
        mark(f"p_v{g}")
        cols = pl.ds(g * vcols, vcols)
        r.yv[theirs, cols] = nn(r.xn[theirs, :], r.wv_v[:, cols]).astype(bf16)
        for hh in range(pair):
            h = g * pair + hh
            state = tn(r.kin[:, keys_of(h)], r.yv[:, values_of(h)]).astype(bf16)
            for lane in range(HEAD_V // LANES):
                tiles = HEAD_K // PIECE_ROWS
                r.st_send[g, pl.ds(lane * tiles, tiles), hh] = state[
                    :, lane * LANES : (lane + 1) * LANES
                ].reshape(tiles, PIECE_ROWS, LANES)
        mark(f"p_asend{g}")
        send_states(g)

    mark("p_qtheir")
    r.yq[theirs, :] = nn(r.xn[theirs, :], r.wq_v[...]).astype(bf16)

    def gates(rows):
        u = nn(r.xn[rows, :], r.wg_v[...]).astype(bf16).astype(f32)
        r.sg[rows, :] = r.hgain_v[...] * (u * (0.5 + 0.5 * jnp.tanh(0.5 * u)))

    mark("p_gown")
    for copy in wg_copies:
        copy.wait()
    gates(own)

    def bulk(ref, ssem, rsem):
        return remote(ref, ref, ssem, rsem, partner)

    def b_copy(g, d):
        return remote(
            r.tot_send.at[g],
            r.tot_recv.at[g, d],
            r.b_send.at[g, d],
            r.b_recv.at[g, d],
            outer_dev(lax.rem(z + d, outer)),
        )

    for g in range(groups):
        mark(f"p_waitA{g}")
        bulk(r.st_recv.at[g, pl.ds(1, inner - 1)], r.a_send.at[g], r.a_recv.at[g]).wait_recv()
        mark(f"p_bsend{g}")
        total = r.st_recv[g, 0].astype(f32)
        for d in range(1, inner):
            total = total + r.st_recv[g, d].astype(f32)
        r.tot_send[g] = total.astype(bf16)
        for d in range(1, outer):

            @pl.when(z + d < outer)
            def _():
                b_copy(g, d).start()

    mark("p_gtheir")
    gates(theirs)

    mark("p_attn")
    for h in range(heads):
        row = log_decay_of(r.bias_v[pl.ds(h, 1), :])
        q_here = (
            r.yq[:, keys_of(h)].astype(f32) * (jnp.exp(row * steps) * HEAD_K ** (-0.5))
        ).astype(bf16)
        r.qin[:, keys_of(h)] = q_here
        v_here = r.yv[:, values_of(h)]
        parts = 2
        rows = span // parts
        for part in range(parts):
            last = (part + 1) * rows
            scores = nt(q_here[part * rows : last], r.kin[pl.ds(0, last), keys_of(h)])
            at = lax.broadcasted_iota(jnp.int32, scores.shape, 0) + part * rows
            to = lax.broadcasted_iota(jnp.int32, scores.shape, 1)
            scores = jnp.where(to <= at, scores, 0.0).astype(bf16)
            r.pv[pl.ds(part * rows, rows), values_of(h)] = nn(scores, v_here[:last])

    for g in range(groups):
        mark(f"p_waitB{g}")
        r.acc[...] = jnp.zeros_like(r.acc)
        for d in range(1, outer):

            @pl.when(z >= d)
            def _():
                b_copy(g, d).wait_recv()
                r.acc[...] += r.tot_recv[g, d].astype(f32)

        mark(f"p_csend{g}")
        carry = r.acc[...]
        for i in range(inner):
            r.c_send[g, i] = carry.astype(bf16)
            if i + 1 < inner:
                carry = carry + r.st_recv[g, lax.rem(p - i + inner, inner)].astype(f32)
        for d in range(1, inner):
            i = lax.rem(p + d, inner)
            remote(
                r.c_send.at[g, i], r.c_recv.at[g, p], r.cs_send.at[g], r.cs_recv.at[g], plane_dev(i)
            ).start()
        r.c_recv[g, p] = r.c_send[g, p]

    for g in range(groups):
        mark(f"p_waitC{g}")
        bulk(r.c_recv.at[g, pl.ds(1, inner - 1)], r.cs_send.at[g], r.cs_recv.at[g]).wait_recv()
        mark(f"p_fin{g}")
        for hh in range(pair):
            h = g * pair + hh
            tiles = HEAD_K // PIECE_ROWS
            state = jnp.concatenate(
                [
                    r.c_recv[g, pl.ds(lane * tiles, tiles), hh].reshape(HEAD_K, LANES)
                    for lane in range(HEAD_V // LANES)
                ],
                axis=1,
            )
            att = r.pv[:, values_of(h)] + nn(r.qin[:, keys_of(h)], state)
            scale = lax.rsqrt(jnp.mean(att * att, axis=-1, keepdims=True) + epsilon)
            r.gated[:, values_of(h)] = (att * scale * r.sg[:, values_of(h)]).astype(bf16)

    tiles = model // OUT_TILE

    def o_copy(t):
        return remote(r.o_send.at[t], r.o_recv.at[t], r.os_send.at[t], r.os_recv.at[t], partner)

    def out_copy(t):
        columns = pl.ds(t * OUT_TILE, OUT_TILE)
        return pltpu.make_async_copy(r.o_buf.at[t], r.out.at[:, columns], r.ob_sem.at[t])

    mark("p_otheirs")
    wo_copy.wait()
    for t in range(tiles):
        columns = pl.ds(t * OUT_TILE, OUT_TILE)
        r.o_send[t] = nn(r.gated[theirs, :], r.wo_v[:, columns]).astype(bf16)
        o_copy(t).start()
    mark("p_oown")
    for t in range(tiles):
        columns = pl.ds(t * OUT_TILE, OUT_TILE)
        part = nn(r.gated[own, :], r.wo_v[:, columns])
        o_copy(t).wait_recv()
        r.o_buf[t] = (part + r.o_recv[t].astype(f32)).astype(bf16)
        out_copy(t).start()

    mark("p_outwait")
    for t in range(tiles):
        o_copy(t).wait_send()
        out_copy(t).wait()
    for g in range(groups):
        bulk(r.st_send.at[g, pl.ds(1, inner - 1)], r.a_send.at[g], r.a_recv.at[g]).wait_send()
        bulk(r.c_send.at[g, pl.ds(1, inner - 1)], r.cs_send.at[g], r.cs_recv.at[g]).wait_send()
        for d in range(1, outer):

            @pl.when(z + d < outer)
            def _():
                b_copy(g, d).wait_send()

    mark(None)


def per_device(sp_count, tokens, norm_gain, wq, wk, wv, wg, decay_bias, head_gain, wo):
    half, model = tokens.shape
    span = 2 * half
    width = wk.shape[1]
    vwidth = wv.shape[1]
    heads = width // HEAD_K
    groups = 2
    pair = heads // groups
    outer = sp_count // PIECES
    tiles = model // OUT_TILE
    piece = (pair, PIECE_ROWS, LANES)
    vm = pltpu.VMEM
    dma = pltpu.SemaphoreType.DMA
    hbm = pl.BlockSpec(memory_space=pltpu.HBM)
    inputs = dict(
        tokens=tokens,
        norm_gain=norm_gain.reshape(1, model),
        wq=wq,
        wk=wk,
        wv=wv,
        wg=wg,
        decay_bias=decay_bias.reshape(heads, HEAD_K),
        head_gain=head_gain.reshape(1, vwidth),
        wo=wo,
    )
    scratch = dict(
        xn=vm((span, model), bf16),
        scale_v=vm((half // TOKEN_CHUNKS, LANES), f32),
        gain_v=vm((1, model), f32),
        bias_v=vm((heads, HEAD_K), f32),
        hgain_v=vm((1, vwidth), f32),
        wk_v=vm((model, width), bf16),
        wq_v=vm((model, width), bf16),
        wv_v=vm((model, vwidth), bf16),
        wg_v=vm((model, vwidth), bf16),
        wo_v=vm((vwidth, model), bf16),
        yk=vm((span, width), bf16),
        yq=vm((span, width), bf16),
        yv=vm((span, vwidth), bf16),
        sg=vm((span, vwidth), f32),
        kin=vm((span, width), bf16),
        qin=vm((span, width), bf16),
        pv=vm((span, vwidth), f32),
        gated=vm((span, vwidth), bf16),
        st_send=vm((groups, PIECES) + piece, bf16),
        st_recv=vm((groups, PIECES) + piece, bf16),
        tot_send=vm((groups,) + piece, bf16),
        tot_recv=vm((groups, outer) + piece, bf16),
        acc=vm(piece, f32),
        c_send=vm((groups, PIECES) + piece, bf16),
        c_recv=vm((groups, PIECES) + piece, bf16),
        o_send=vm((tiles, half, OUT_TILE), bf16),
        o_recv=vm((tiles, half, OUT_TILE), bf16),
        o_buf=vm((tiles, half, OUT_TILE), bf16),
        tok_sem=dma((TOKEN_CHUNKS,)),
        small_sem=dma((3,)),
        w_sem=dma((2 + 2 * groups,)),
        wo_sem=dma,
        tok_send=dma,
        tok_recv=dma,
        a_send=dma((groups,)),
        a_recv=dma((groups,)),
        b_send=dma((groups, outer)),
        b_recv=dma((groups, outer)),
        cs_send=dma((groups,)),
        cs_recv=dma((groups,)),
        os_send=dma((tiles,)),
        os_recv=dma((tiles,)),
        ob_sem=dma((tiles,)),
    )
    names = tuple(inputs) + ("out",) + tuple(scratch)
    return pl.pallas_call(
        functools.partial(kernel, sp_count, names),
        out_shape=jax.ShapeDtypeStruct((half, model), bf16),
        in_specs=[hbm] * len(inputs),
        out_specs=hbm,
        scratch_shapes=list(scratch.values()),
        compiler_params=pltpu.CompilerParams(
            collective_id=0, has_side_effects=True, vmem_limit_bytes=VMEM_BYTES
        ),
    )(*inputs.values())


def solution(mesh):
    return jax.shard_map(
        functools.partial(per_device, mesh.shape["sp"]),
        mesh=mesh,
        in_specs=(
            P(("sp", "tp"), None),
            P(),
            P(None, "tp"),
            P(None, "tp"),
            P(None, "tp"),
            P(None, "tp"),
            P("tp"),
            P("tp"),
            P("tp", None),
        ),
        out_specs=P(("sp", "tp"), None),
        check_vma=False,
    )
```

time: 59.4 us -> 46.7 us (0.79)
  the two profiles are of different devices: /device:TPU:120 before, /device:TPU:1 now
where the time goes in v1:
time: 46.7 us; the launch traced here: 45.8 us
  Pallas kernels  42.7 us (91%)
  local copies, waits for them, and re-layouts  3.13 us (7%)
    pallas_call x1, Pallas kernels, per_device(): pl.pallas_call(functools.partial(kernel, sp_count, names), out_shape=jax....  42.7 us
    unnamed x1, local copies, waits for them, and re-layouts  3.13 us

profile of v1, /device:TPU:1, one launch (start us, length us, event | category | flops | bytes accessed | tf_op | source)
XLA Modules:
  0.0 45.8 jit_solution(9010256565571140736)
XLA Ops:
  0.0 42.7 %shard_map.91 = bf16[256,4096]{1,0:T(8,128)(2,1)} custom-call(bf16[256,4096]{1,0:T(8,128)(2,1)} %refs_0_.1, f32[1,4096]{1,0:T(1,128)} %bitcast.3, bf16[4096,512]{1,0:T(8,128)(2,1)} %refs_2_.1, bf16[4096,512]{1,0:T(8,128)(2,1)} %refs_3_.1, bf16[4096,1024]{1,0:T(8,128)(2,1)} %refs_4_.1, bf16[4096,1024]{1,0:T(8,128)(2,1)} %refs_5_.1, f32[4,128]{1,0:T(4,128)} %bitcast.5, ...), custom_call_target="tpu_custom_call" | custom-call | tf_op jit(solution)/shard_map/pallas_call | solution.py:418
  42.7 3.1 %copy.11 = bf16[256,4096]{1,0:T(8,128)(2,1)} copy(bf16[256,4096]{1,0:T(8,128)(2,1)} %shard_map.91) | data formatting | bytes 4194304

commit v2 on v1

--- a/solution.py
+++ b/solution.py
@@ -20,9 +20,9 @@
 MESH = pl.DeviceIdType.MESH
 f32 = jnp.float32
 bf16 = jnp.bfloat16
-OUT_TILE = 512
 TOKEN_CHUNKS = 4
-VMEM_BYTES = 67_000_000
+SEND_CHUNKS = 2
+VMEM_BYTES = 62_500_000
 
 
 def nn(a, b):
@@ -81,9 +81,8 @@
     tok_copies = []
     for i in range(TOKEN_CHUNKS):
         rows = pl.ds(i * chunk, chunk)
-        mine = pl.ds(pl.multiple_of(c * half + i * chunk, chunk), chunk)
         tok_copies.append(
-            pltpu.make_async_copy(r.tokens.at[rows, :], r.xn.at[mine, :], r.tok_sem.at[i])
+            pltpu.make_async_copy(r.tokens.at[rows, :], r.xraw.at[rows, :], r.tok_sem.at[i])
         )
     small = [
         pltpu.make_async_copy(r.norm_gain, r.gain_v, r.small_sem.at[0]),
@@ -104,11 +103,7 @@
             )
         )
     wo_copy = pltpu.make_async_copy(r.wo, r.wo_v, r.wo_sem)
-    tok_copies[0].start()
-    small[0].start()
-    for copy in tok_copies[1:]:
-        copy.start()
-    for copy in [wk_copy] + wv_copies + [wq_copy] + small[1:] + wg_copies + [wo_copy]:
+    for copy in tok_copies + small[:1]:
         copy.start()
 
     barrier = pltpu.get_barrier_semaphore()
@@ -122,46 +117,46 @@
             barrier, inc=1, device_id=outer_dev(lax.rem(z + d, outer)), device_id_type=MESH
         )
 
+    wk_copy.start()
     mark("p_norm")
     sub = 16
     small[0].wait()
     for i in range(TOKEN_CHUNKS):
         tok_copies[i].wait()
-        first = c * half + i * chunk
+        if i + 1 == TOKEN_CHUNKS:
+            for copy in wv_copies + small[1:]:
+                copy.start()
 
         @pl.loop(0, chunk // sub, unroll=True)
         def _(k):
-            rows = pl.ds(pl.multiple_of(first + k * sub, sub), sub)
-            x = r.xn[rows, :].astype(f32)
+            x = r.xraw[pl.ds(i * chunk + k * sub, sub), :].astype(f32)
             scale = lax.rsqrt(jnp.mean(x * x, axis=-1, keepdims=True) + epsilon)
-            r.scale_v[pl.ds(k * sub, sub), :] = jnp.broadcast_to(scale, (sub, LANES))
-
-        @pl.loop(0, chunk // sub)
-        def _(k):
-            rows = pl.ds(pl.multiple_of(first + k * sub, sub), sub)
-            x = r.xn[rows, :].astype(f32)
-            scale = r.scale_v[pl.ds(pl.multiple_of(k * sub, sub), sub), pl.ds(0, 1)]
+            rows = pl.ds(pl.multiple_of(c * half + i * chunk + k * sub, sub), sub)
             r.xn[rows, :] = (x * scale * r.gain_v[...]).astype(bf16)
 
     mark("p_barrier")
     pl.semaphore_wait(barrier, inner + outer - 1)
-    send_tok = remote(r.xn.at[own, :], r.xn.at[own, :], r.tok_send, r.tok_recv, partner)
-    send_tok.start()
-
+    part_rows = half // SEND_CHUNKS
+    tok_sends = []
+    for i in range(SEND_CHUNKS):
+        rows = pl.ds(pl.multiple_of(c * half + i * part_rows, part_rows), part_rows)
+        tok_sends.append(
+            remote(r.xn.at[rows, :], r.xn.at[rows, :], r.tok_send.at[i], r.tok_recv.at[i], partner)
+        )
+        tok_sends[-1].start()
     mark("p_kown")
     wk_copy.wait()
     r.yk[own, :] = nn(r.xn[own, :], r.wk_v[...]).astype(bf16)
     mark("p_vown")
-    for copy in wv_copies:
-        copy.wait()
-    r.yv[own, :] = nn(r.xn[own, :], r.wv_v[...]).astype(bf16)
-    mark("p_qown")
-    wq_copy.wait()
-    r.yq[own, :] = nn(r.xn[own, :], r.wq_v[...]).astype(bf16)
-    mark("p_waittok")
     for copy in small[1:]:
         copy.wait()
-    send_tok.wait()
+    for g in range(groups):
+        cols = pl.ds(g * vcols, vcols)
+        wv_copies[g].wait()
+        r.yv[own, cols] = nn(r.xn[own, :], r.wv_v[:, cols]).astype(bf16)
+    for copy in [wq_copy] + wg_copies + [wo_copy]:
+        copy.start()
+    mark("p_stown")
 
     def log_decay_of(bias):
         return -jnp.log1p(jnp.exp(-(bias + math.log(sp_count * span / 8.0)))) / decay_power
@@ -174,13 +169,19 @@
     def keys_of(h):
         return pl.ds(h * HEAD_K, HEAD_K)
 
-    mark("p_ktheir")
-    r.yk[theirs, :] = nn(r.xn[theirs, :], r.wk_v[...]).astype(bf16)
+    def decayed_keys(rows, h):
+        row = log_decay_of(r.bias_v[pl.ds(h, 1), :])
+        first = (s * span + 1 + (c if rows is own else other) * half).astype(f32)
+        steps_here = lax.broadcasted_iota(jnp.int32, (half, HEAD_K), 0).astype(f32) + first
+        keys = r.yk[rows, keys_of(h)].astype(f32) * jnp.exp(-row * steps_here)
+        r.kin[rows, keys_of(h)] = keys.astype(bf16)
+        return tn(keys.astype(bf16), r.yv[rows, values_of(h)])
+
     for h in range(heads):
-        row = log_decay_of(r.bias_v[pl.ds(h, 1), :])
-        r.kin[:, keys_of(h)] = (r.yk[:, keys_of(h)].astype(f32) * jnp.exp(-row * steps)).astype(
-            bf16
-        )
+        r.st_acc[h] = decayed_keys(own, h)
+    mark("p_waittok")
+    for copy in tok_sends:
+        copy.wait_recv()
 
     def send_states(g):
         for d in range(1, inner):
@@ -190,13 +191,15 @@
             ).start()
         r.st_recv[g, 0] = r.st_send[g, p]
 
+    mark("p_ktheir")
+    r.yk[theirs, :] = nn(r.xn[theirs, :], r.wk_v[...]).astype(bf16)
     for g in range(groups):
-        mark(f"p_v{g}")
-        cols = pl.ds(g * vcols, vcols)
-        r.yv[theirs, cols] = nn(r.xn[theirs, :], r.wv_v[:, cols]).astype(bf16)
+        mark(f"p_kv{g}")
+        vcols_g = pl.ds(g * vcols, vcols)
+        r.yv[theirs, vcols_g] = nn(r.xn[theirs, :], r.wv_v[:, vcols_g]).astype(bf16)
         for hh in range(pair):
             h = g * pair + hh
-            state = tn(r.kin[:, keys_of(h)], r.yv[:, values_of(h)]).astype(bf16)
+            state = (r.st_acc[h] + decayed_keys(theirs, h)).astype(bf16)
             for lane in range(HEAD_V // LANES):
                 tiles = HEAD_K // PIECE_ROWS
                 r.st_send[g, pl.ds(lane * tiles, tiles), hh] = state[
@@ -205,17 +208,10 @@
         mark(f"p_asend{g}")
         send_states(g)
 
-    mark("p_qtheir")
-    r.yq[theirs, :] = nn(r.xn[theirs, :], r.wq_v[...]).astype(bf16)
-
-    def gates(rows):
-        u = nn(r.xn[rows, :], r.wg_v[...]).astype(bf16).astype(f32)
-        r.sg[rows, :] = r.hgain_v[...] * (u * (0.5 + 0.5 * jnp.tanh(0.5 * u)))
-
-    mark("p_gown")
-    for copy in wg_copies:
-        copy.wait()
-    gates(own)
+    def gates(rows, g):
+        cols = pl.ds(g * vcols, vcols)
+        u = nn(r.xn[rows, :], r.wg_v[:, cols]).astype(bf16).astype(f32)
+        r.sg[rows, cols] = r.hgain_v[:, cols] * (u * (0.5 + 0.5 * jnp.tanh(0.5 * u)))
 
     def bulk(ref, ssem, rsem):
         return remote(ref, ref, ssem, rsem, partner)
@@ -229,7 +225,7 @@
             outer_dev(lax.rem(z + d, outer)),
         )
 
-    for g in range(groups):
+    def reduce_states(g):
         mark(f"p_waitA{g}")
         bulk(r.st_recv.at[g, pl.ds(1, inner - 1)], r.a_send.at[g], r.a_recv.at[g]).wait_recv()
         mark(f"p_bsend{g}")
@@ -243,11 +239,7 @@
             def _():
                 b_copy(g, d).start()
 
-    mark("p_gtheir")
-    gates(theirs)
-
-    mark("p_attn")
-    for h in range(heads):
+    def local_part(h):
         row = log_decay_of(r.bias_v[pl.ds(h, 1), :])
         q_here = (
             r.yq[:, keys_of(h)].astype(f32) * (jnp.exp(row * steps) * HEAD_K ** (-0.5))
@@ -264,7 +256,7 @@
             scores = jnp.where(to <= at, scores, 0.0).astype(bf16)
             r.pv[pl.ds(part * rows, rows), values_of(h)] = nn(scores, v_here[:last])
 
-    for g in range(groups):
+    def send_carries(g):
         mark(f"p_waitB{g}")
         r.acc[...] = jnp.zeros_like(r.acc)
         for d in range(1, outer):
@@ -287,7 +279,7 @@
             ).start()
         r.c_recv[g, p] = r.c_send[g, p]
 
-    for g in range(groups):
+    def finish_heads(g):
         mark(f"p_waitC{g}")
         bulk(r.c_recv.at[g, pl.ds(1, inner - 1)], r.cs_send.at[g], r.cs_recv.at[g]).wait_recv()
         mark(f"p_fin{g}")
@@ -305,33 +297,67 @@
             scale = lax.rsqrt(jnp.mean(att * att, axis=-1, keepdims=True) + epsilon)
             r.gated[:, values_of(h)] = (att * scale * r.sg[:, values_of(h)]).astype(bf16)
 
-    tiles = model // OUT_TILE
-
-    def o_copy(t):
-        return remote(r.o_send.at[t], r.o_recv.at[t], r.os_send.at[t], r.os_recv.at[t], partner)
-
-    def out_copy(t):
-        columns = pl.ds(t * OUT_TILE, OUT_TILE)
-        return pltpu.make_async_copy(r.o_buf.at[t], r.out.at[:, columns], r.ob_sem.at[t])
-
-    mark("p_otheirs")
+    mark("p_q")
+    wq_copy.wait()
+    r.yq[...] = nn(r.xn[...], r.wq_v[...]).astype(bf16)
+    mark("p_g0own")
+    wg_copies[0].wait()
+    gates(own, 0)
+    reduce_states(0)
+    mark("p_g1own")
+    wg_copies[1].wait()
+    gates(own, 1)
+    reduce_states(1)
+    mark("p_g0their")
+    gates(theirs, 0)
+    mark("p_attn0")
+    for h in range(pair):
+        local_part(h)
+    send_carries(0)
+    mark("p_g1their")
+    gates(theirs, 1)
+    send_carries(1)
+    mark("p_attn1")
+    for h in range(pair, heads):
+        local_part(h)
     wo_copy.wait()
-    for t in range(tiles):
-        columns = pl.ds(t * OUT_TILE, OUT_TILE)
-        r.o_send[t] = nn(r.gated[theirs, :], r.wo_v[:, columns]).astype(bf16)
-        o_copy(t).start()
+
+    finish_heads(0)
+    mark("p_o0")
+    low = pl.ds(0, vcols)
+    high = pl.ds(vcols, vcols)
+    r.part_t[...] = nn(r.gated[theirs, low], r.wo_v[low, :])
+    r.part_o[...] = nn(r.gated[own, low], r.wo_v[low, :])
+    finish_heads(1)
+    ncols = model // 2
+
+    def o_copy(n):
+        dst = r.recv0 if n == 0 else r.recv1
+        return remote(r.xraw.at[:, pl.ds(n * ncols, ncols)], dst, r.os_send.at[n], r.os_recv.at[n], partner)
+
+    for n in range(2):
+        mark(f"p_otheirs{n}")
+        columns = pl.ds(n * ncols, ncols)
+        r.xraw[:, columns] = (
+            r.part_t[:, columns] + nn(r.gated[theirs, high], r.wo_v[high, columns])
+        ).astype(bf16)
+        o_copy(n).start()
     mark("p_oown")
-    for t in range(tiles):
-        columns = pl.ds(t * OUT_TILE, OUT_TILE)
-        part = nn(r.gated[own, :], r.wo_v[:, columns])
-        o_copy(t).wait_recv()
-        r.o_buf[t] = (part + r.o_recv[t].astype(f32)).astype(bf16)
-        out_copy(t).start()
-
-    mark("p_outwait")
-    for t in range(tiles):
-        o_copy(t).wait_send()
-        out_copy(t).wait()
+    left = pl.ds(0, ncols)
+    right = pl.ds(ncols, ncols)
+    r.part_o[:, left] += nn(r.gated[own, high], r.wo_v[high, left])
+    mark("p_wait0")
+    o_copy(0).wait_recv()
+    mark("p_oown1")
+    r.part1[...] = r.part_o[:, right] + nn(r.gated[own, high], r.wo_v[high, right])
+    r.res0[...] = (r.part_o[:, left] + r.recv0[...].astype(f32)).astype(bf16)
+    mark("p_wait1")
+    o_copy(1).wait_recv()
+    mark("p_drain")
+    for n in range(2):
+        o_copy(n).wait_send()
+    for copy in tok_sends:
+        copy.wait_send()
     for g in range(groups):
         bulk(r.st_send.at[g, pl.ds(1, inner - 1)], r.a_send.at[g], r.a_recv.at[g]).wait_send()
         bulk(r.c_send.at[g, pl.ds(1, inner - 1)], r.cs_send.at[g], r.cs_recv.at[g]).wait_send()
@@ -342,6 +368,17 @@
                 b_copy(g, d).wait_send()
 
     mark(None)
+
+
+def write_out(res0, part1, recv1, out, buf, sem):
+    cols = res0.shape[1]
+    left = pltpu.make_async_copy(res0, out.at[:, pl.ds(0, cols)], sem.at[0])
+    right = pltpu.make_async_copy(buf, out.at[:, pl.ds(cols, cols)], sem.at[1])
+    left.start()
+    buf[...] = (part1[...] + recv1[...].astype(f32)).astype(bf16)
+    right.start()
+    left.wait()
+    right.wait()
 
 
 def per_device(sp_count, tokens, norm_gain, wq, wk, wv, wg, decay_bias, head_gain, wo):
@@ -353,7 +390,6 @@
     groups = 2
     pair = heads // groups
     outer = sp_count // PIECES
-    tiles = model // OUT_TILE
     piece = (pair, PIECE_ROWS, LANES)
     vm = pltpu.VMEM
     dma = pltpu.SemaphoreType.DMA
@@ -371,7 +407,7 @@
     )
     scratch = dict(
         xn=vm((span, model), bf16),
-        scale_v=vm((half // TOKEN_CHUNKS, LANES), f32),
+        xraw=vm((half, model), bf16),
         gain_v=vm((1, model), f32),
         bias_v=vm((heads, HEAD_K), f32),
         hgain_v=vm((1, vwidth), f32),
@@ -395,36 +431,50 @@
         acc=vm(piece, f32),
         c_send=vm((groups, PIECES) + piece, bf16),
         c_recv=vm((groups, PIECES) + piece, bf16),
-        o_send=vm((tiles, half, OUT_TILE), bf16),
-        o_recv=vm((tiles, half, OUT_TILE), bf16),
-        o_buf=vm((tiles, half, OUT_TILE), bf16),
+        st_acc=vm((heads, HEAD_K, HEAD_V), f32),
+        recv0=vm((half, model // 2), bf16),
+        part_t=vm((half, model), f32),
+        part_o=vm((half, model), f32),
         tok_sem=dma((TOKEN_CHUNKS,)),
         small_sem=dma((3,)),
         w_sem=dma((2 + 2 * groups,)),
         wo_sem=dma,
-        tok_send=dma,
-        tok_recv=dma,
+        tok_send=dma((SEND_CHUNKS,)),
+        tok_recv=dma((SEND_CHUNKS,)),
         a_send=dma((groups,)),
         a_recv=dma((groups,)),
         b_send=dma((groups, outer)),
         b_recv=dma((groups, outer)),
         cs_send=dma((groups,)),
         cs_recv=dma((groups,)),
-        os_send=dma((tiles,)),
-        os_recv=dma((tiles,)),
-        ob_sem=dma((tiles,)),
+        os_send=dma((2,)),
+        os_recv=dma((2,)),
     )
-    names = tuple(inputs) + ("out",) + tuple(scratch)
-    return pl.pallas_call(
+    outs = dict(
+        res0=vm((half, model // 2), bf16),
+        part1=vm((half, model // 2), f32),
+        recv1=vm((half, model // 2), bf16),
+    )
+    names = tuple(inputs) + tuple(outs) + tuple(scratch)
+    vmem = pl.BlockSpec(memory_space=pltpu.VMEM)
+    parts = pl.pallas_call(
         functools.partial(kernel, sp_count, names),
-        out_shape=jax.ShapeDtypeStruct((half, model), bf16),
+        out_shape=tuple(outs.values()),
         in_specs=[hbm] * len(inputs),
-        out_specs=hbm,
+        out_specs=(vmem,) * len(outs),
         scratch_shapes=list(scratch.values()),
         compiler_params=pltpu.CompilerParams(
             collective_id=0, has_side_effects=True, vmem_limit_bytes=VMEM_BYTES
         ),
     )(*inputs.values())
+    return pl.pallas_call(
+        write_out,
+        out_shape=jax.ShapeDtypeStruct((half, model), bf16),
+        in_specs=[vmem] * len(outs),
+        out_specs=hbm,
+        scratch_shapes=[vm((half, model // 2), bf16), dma((2,))],
+        compiler_params=pltpu.CompilerParams(vmem_limit_bytes=16_000_000),
+    )(*[pltpu.with_memory_space_constraint(x, pltpu.VMEM) for x in parts])
 
 
 def solution(mesh):

time: 46.7 us -> 38.3 us (0.82); the launches traced: 45.8 us -> 38.2 us
  Pallas kernels: 42.7 us -> 38 us
  local copies, waits for them, and re-layouts: 3.13 us -> 0 us
    pallas_call x1 -> x2, Pallas kernels: 42.7 us -> 38 us  [the longest x1 36.7 us: per_device(): pl.pallas_call(functools.partial(kernel, sp_count, names), out_shape=tupl...]
    unnamed x1 -> x0, local copies, waits for them, and re-layouts: 3.13 us -> none
where the time goes in v2:
time: 38.3 us; the launch traced here: 38.2 us
  Pallas kernels  38 us (99%)
    pallas_call x1, Pallas kernels, per_device(): pl.pallas_call(functools.partial(kernel, sp_count, names), out_shape=tupl...  36.7 us
    pallas_call x1, Pallas kernels, per_device(): pl.pallas_call(write_out, out_shape=jax.ShapeDtypeStruct((half, model), b...  1.34 us

profile of v2, /device:TPU:1, one launch (start us, length us, event | category | flops | bytes accessed | tf_op | source)
XLA Modules:
  0.0 38.2 jit_solution(14684837666659152951)
XLA Ops:
  0.0 36.7 %shard_map.91 = (bf16[256,2048]{1,0:T(8,128)(2,1)S(1)}, f32[256,2048]{1,0:T(8,128)S(1)}, bf16[256,2048]{1,0:T(8,128)(2,1)S(1)}) custom-call(bf16[256,4096]{1,0:T(8,128)(2,1)} %refs_0_.1, f32[1,4096]{1,0:T(1,128)} %bitcast.3, bf16[4096,512]{1,0:T(8,128)(2,1)} %refs_2_.1, bf16[4096,512]{1,0:T(8,128)(2,1)} %refs_3_.1, bf16[4096,1024]{1,0:T(8,128)(2,1)} %refs_4_.1, ...), custom_call_target="tpu_custom_call" | custom-call | tf_op jit(solution)/shard_map/pallas_call | solution.py:460
  36.7 1.3 %shard_map.92 = bf16[256,4096]{1,0:T(8,128)(2,1)} custom-call(bf16[256,2048]{1,0:T(8,128)(2,1)S(1)} %get-tuple-element.8.res0, f32[256,2048]{1,0:T(8,128)S(1)} %get-tuple-element.9.part1, bf16[256,2048]{1,0:T(8,128)(2,1)S(1)} %get-tuple-element.10.recv1), custom_call_target="tpu_custom_call" | custom-call | tf_op jit(solution)/shard_map/pallas_call | solution.py:470
